TPU v7x, 32 devices: a whole 2x2x4 slice. The times are simulated.
32 devices in a mesh: fs: 8 (over z, y), tp: 4 (over x, core).
Axes of the slice: x: 2, y: 2, z: 4, core: 2. Of those that a mesh axis runs over, the one named last changes fastest.
Arguments:
- stream_in: bfloat16 [2048, 2112], P('fs'), may hold values from -6 to 6
- norm_gains: float32 [6, 2112], replicated, may hold values from 0.1 to 1.9
- gate_proj: bfloat16 [2112, 3072], P('fs', 'tp'), may hold values from -0.125 to 0.125
- up_proj: bfloat16 [2112, 3072], P('fs', 'tp'), may hold values from -0.125 to 0.125
- down_proj: bfloat16 [2112, 3072], P('fs', 'tp'), may hold values from -0.109375 to 0.109375
- outer_gate: bfloat16 [2112, 1056], P('fs', 'tp'), may hold values from -0.125 to 0.125
- inner_gate: bfloat16 [2112, 1056], P('fs', 'tp'), may hold values from -0.125 to 0.125
- value_proj: bfloat16 [2112, 1056], P('fs', 'tp'), may hold values from -0.125 to 0.125
- mixer_out: bfloat16 [2112, 1056], P('fs', 'tp'), may hold values from -0.1875 to 0.1875
- conv_taps: bfloat16 [3, 1056], replicated, may hold values from -3 to 3
Outputs:
- stream_out: bfloat16 [2048, 2112], P('fs')
All inputs are finite; a program needn't handle non-finite values.
Results may differ from a plain program's by a relative error of at most 0.02.
Values may be sent and summed in bfloat16 or wider, within the bound.
A program may use at most 64 MiB of HBM per device.

v0:
```python
import jax
import jax.numpy as jnp
from jax import lax
from jax.sharding import PartitionSpec as P

CONV_K = 3
EPSILON = 1e-06


def scaled(values, gain):
    return values * lax.rsqrt(jnp.mean(values * values, axis=-1, keepdims=True) + EPSILON) * gain


def narrow(inner, weight, stream, gain, factor):
    partial_value = lax.dot_general(
        inner, weight, (((1,), (1,)), ((), ())), preferred_element_type=jnp.float32
    )
    summed = lax.psum(partial_value.astype(jnp.bfloat16), "tp").astype(jnp.float32)
    return (stream.astype(jnp.float32) + factor * scaled(summed, gain)).astype(jnp.bfloat16)


def half_step(stream, weights, pre_gain, post_gain):
    gate_full, up_full, down_full = weights
    normed = scaled(stream.astype(jnp.float32), pre_gain).astype(jnp.bfloat16)
    gate = jnp.dot(normed, gate_full, preferred_element_type=jnp.float32)
    upward = jnp.dot(normed, up_full, preferred_element_type=jnp.float32)
    hidden = (jax.nn.silu(gate) * upward).astype(jnp.bfloat16)
    return narrow(hidden, down_full, stream, post_gain, 0.5)


def mixer_step(stream, weights, conv_taps, pre_gain, post_gain):
    outer_full, inner_full, value_full, out_full = weights
    channels = outer_full.shape[1]
    normed = scaled(stream.astype(jnp.float32), pre_gain).astype(jnp.bfloat16)
    outer = (
        jnp.dot(normed, outer_full, preferred_element_type=jnp.float32)
        .astype(jnp.bfloat16)
        .astype(jnp.float32)
    )
    inner = (
        jnp.dot(normed, inner_full, preferred_element_type=jnp.float32)
        .astype(jnp.bfloat16)
        .astype(jnp.float32)
    )
    value = (
        jnp.dot(normed, value_full, preferred_element_type=jnp.float32)
        .astype(jnp.bfloat16)
        .astype(jnp.float32)
    )
    gated = inner * value
    taps = lax.dynamic_slice_in_dim(conv_taps, lax.axis_index("tp") * channels, channels, 1).astype(
        jnp.float32
    )
    length = gated.shape[0]
    padded = jnp.concatenate([jnp.zeros((CONV_K - 1, channels), jnp.float32), gated], axis=0)
    conv = jnp.zeros_like(gated)
    for offset in range(CONV_K):
        conv = conv + taps[offset] * padded[offset : offset + length]
    mixed = (outer * conv).astype(jnp.bfloat16)
    return narrow(mixed, out_full, stream, post_gain, 1.0)


def local(
    stream_in,
    norm_gains,
    gate_proj,
    up_proj,
    down_proj,
    outer_gate,
    inner_gate,
    value_proj,
    mixer_out,
    conv_taps,
):
    mlp_full = (
        lax.all_gather(gate_proj, "fs", axis=0, tiled=True),
        lax.all_gather(up_proj, "fs", axis=0, tiled=True),
        lax.all_gather(down_proj, "fs", axis=0, tiled=True),
    )
    mixer_full = None
    stream = half_step(stream_in, mlp_full, norm_gains[0], norm_gains[1])
    mixer_full = (
        lax.all_gather(outer_gate, "fs", axis=0, tiled=True),
        lax.all_gather(inner_gate, "fs", axis=0, tiled=True),
        lax.all_gather(value_proj, "fs", axis=0, tiled=True),
        lax.all_gather(mixer_out, "fs", axis=0, tiled=True),
    )
    stream = mixer_step(stream, mixer_full, conv_taps, norm_gains[2], norm_gains[3])
    return half_step(stream, mlp_full, norm_gains[4], norm_gains[5])


def solution(mesh):
    return jax.shard_map(
        local,
        mesh=mesh,
        in_specs=(
            P("fs", None),
            P(),
            P("fs", "tp"),
            P("fs", "tp"),
            P("fs", "tp"),
            P("fs", "tp"),
            P("fs", "tp"),
            P("fs", "tp"),
            P("fs", "tp"),
            P(),
        ),
        out_specs=P("fs", None),
        check_vma=False,
    )
```

profile of v0, /device:TPU:0, one launch (start us, length us, event | category | flops | bytes accessed | tf_op | source)
XLA Modules:
  0.0 522.5 jit_solution(16457004554758750413)
XLA Ops:
  6.5 0.7 all-gather.8.cloned.1.call-update
  7.3 0.7 all-gather.10.cloned.1.call-update
  8.1 0.7 all-gather.12.cloned.1.call-update
  8.8 1.4 slice_reduce_fusion
  10.2 1.6 fusion.8
  11.8 61.5 %all-gather.8.cloned.1.call-done = bf16[2112,768]{1,0:T(8,128)(2,1)} async-done(((bf16[264,768]{1,0:T(8,128)(2,1)}), bf16[2112,768]{1,0:T(8,128)(2,1)}) %all-gather.8.cloned.1.call-update) | async-done | bytes 3244048 | tf_op jit(solution)/shard_map/all_gather | solution.py:76
  73.3 3.2 fusion.36
  76.6 58.7 %all-gather.10.cloned.1.call-done = bf16[2112,768]{1,0:T(8,128)(2,1)} async-done(((bf16[264,768]{1,0:T(8,128)(2,1)}), bf16[2112,768]{1,0:T(8,128)(2,1)}) %all-gather.10.cloned.1.call-update) | async-done | bytes 3244048 | tf_op jit(solution)/shard_map/all_gather | solution.py:77
  135.3 62.0 %all-gather.12.cloned.1.call-done = bf16[2112,768]{1,0:T(8,128)(2,1)} async-done(((bf16[264,768]{1,0:T(8,128)(2,1)}), bf16[2112,768]{1,0:T(8,128)(2,1)}) %all-gather.12.cloned.1.call-update) | async-done | bytes 3244048 | tf_op jit(solution)/shard_map/all_gather | solution.py:78
  197.2 6.6 %convolution_convert_fusion.2 = bf16[256,2112]{0,1:T(8,128)(2,1)} fusion(bf16[2112,768]{1,0:T(8,128)(2,1)} %all-gather.12.cloned.1.call-done, bf16[2112,768]{1,0:T(8,128)(2,1)} %all-gather.10.cloned.1.call-done, f32[256,768]{1,0:T(8,128)S(1)} %fusion.36, bf16[256,2112]{0,1:T(8,128)(2,1)S(1)} %copy-done, f32[2112]{0:T(1024)S(1)} %get-tuple-element.9, ...), kind=kOutput, calls=%fused_computation.2 | convolution fusion | flops 1664827392 | bytes 9446656 | tf_op jit(solution)/shard_map/dot_general | solution.py:15
  203.9 0.5 all-gather.16.cloned.1.call-update
  205.1 0.7 all-gather.14.cloned.1.call-update
  205.8 0.7 all-gather.20.cloned.1.call-update
  206.6 0.8 dynamic-slice_convert_fusion
  207.4 32.0 %all-reduce.5.cloned.1.call-done = bf16[256,2112]{0,1:T(8,128)(2,1)} async-done(((bf16[256,2112]{0,1:T(8,128)(2,1)}), bf16[256,2112]{0,1:T(8,128)(2,1)}) %all-reduce.5.cloned.1.call-update) | async-done | bytes 1081360 | tf_op jit(solution)/shard_map/psum | solution.py:18
  239.4 1.5 fusion
  241.0 1.9 fusion.12
  242.9 43.7 %all-gather.16.cloned.1.call-done = bf16[2112,264]{1,0:T(8,128)(2,1)} async-done(((bf16[264,264]{1,0:T(8,128)(2,1)}), bf16[2112,264]{1,0:T(8,128)(2,1)}) %all-gather.16.cloned.1.call-update) | async-done | bytes 1115152 | tf_op jit(solution)/shard_map/all_gather | solution.py:84
  286.6 2.5 fusion.24
  289.0 42.7 %all-gather.18.cloned.1.call-done = bf16[2112,264]{1,0:T(8,128)(2,1)} async-done(((bf16[264,264]{1,0:T(8,128)(2,1)}), bf16[2112,264]{1,0:T(8,128)(2,1)}) %all-gather.18.cloned.1.call-update) | async-done | bytes 1115152 | tf_op jit(solution)/shard_map/all_gather | solution.py:85
  331.7 2.5 fusion.23
  334.2 42.9 %all-gather.14.cloned.1.call-done = bf16[2112,264]{1,0:T(8,128)(2,1)} async-done(((bf16[264,264]{1,0:T(8,128)(2,1)}), bf16[2112,264]{1,0:T(8,128)(2,1)}) %all-gather.14.cloned.1.call-update) | async-done | bytes 1115152 | tf_op jit(solution)/shard_map/all_gather | solution.py:83
  377.1 45.3 %all-gather.20.cloned.1.call-done = bf16[2112,264]{1,0:T(8,128)(2,1)} async-done(((bf16[264,264]{1,0:T(8,128)(2,1)}), bf16[2112,264]{1,0:T(8,128)(2,1)}) %all-gather.20.cloned.1.call-update) | async-done | bytes 1115152 | tf_op jit(solution)/shard_map/all_gather | solution.py:86
  422.4 5.0 convolution_convert_fusion.1
  427.6 35.0 %all-reduce.7.cloned.1.call-done = bf16[256,2112]{0,1:T(8,128)(2,1)} async-done(((bf16[256,2112]{0,1:T(8,128)(2,1)}), bf16[256,2112]{0,1:T(8,128)(2,1)}) %all-reduce.7.cloned.1.call-update) | async-done | bytes 1081360 | tf_op jit(solution)/shard_map/psum | solution.py:18
  462.6 1.7 fusion.3
  464.3 1.8 fusion.16
  466.1 1.4 fusion.32
  467.5 6.6 %convolution_convert_fusion = bf16[256,2112]{0,1:T(8,128)(2,1)} fusion(bf16[2112,768]{1,0:T(8,128)(2,1)} %all-gather.12.cloned.1.call-done, bf16[2112,768]{1,0:T(8,128)(2,1)} %all-gather.10.cloned.1.call-done, f32[256,768]{1,0:T(8,128)S(1)} %fusion.32, bf16[256,2112]{0,1:T(8,128)(2,1)S(1)} %get-tuple-element.15, f32[2112]{0:T(1024)S(1)} %get-tuple-element.10, ...), kind=kOutput, calls=%fused_computation | convolution fusion | flops 1664827392 | bytes 9446656 | tf_op jit(solution)/shard_map/dot_general | solution.py:15
  474.1 37.2 %all-reduce.9.cloned.1.call-done = bf16[256,2112]{0,1:T(8,128)(2,1)} async-done(((bf16[256,2112]{0,1:T(8,128)(2,1)}), bf16[256,2112]{0,1:T(8,128)(2,1)}) %all-reduce.9.cloned.1.call-update) | async-done | bytes 1081360 | tf_op jit(solution)/shard_map/psum | solution.py:18
  511.3 1.5 fusion.5
  512.9 2.7 fusion.19
  (25 shorter events, 1.2 us)
Async XLA Ops:
  6.5 66.8 %copy-start = (bf16[256,2112]{0,1:T(8,128)(2,1)S(1)}, bf16[256,2112]{0,1:T(8,128)(2,1)}, u32[]{:S(2)}) copy-start(bf16[256,2112]{0,1:T(8,128)(2,1)} %param.10) | copy-start | bytes 3244036
  6.5 66.8 %all-gather.8.cloned.1.call-start = ((), (), s32[]{:S(2)}) async-start(), calls=%async_computation | async-start | bytes 3649536 | tf_op jit(solution)/shard_map/all_gather | solution.py:76
  7.3 128.0 %all-gather.10.cloned.1.call-start = ((), (), s32[]{:S(2)}) async-start(), calls=%async_computation.1 | async-start | bytes 3649536 | tf_op jit(solution)/shard_map/all_gather | solution.py:77
  8.0 189.2 %all-gather.12.cloned.1.call-start = ((), (), s32[]{:S(2)}) async-start(), calls=%async_computation.2 | async-start | bytes 3649536 | tf_op jit(solution)/shard_map/all_gather | solution.py:78
  8.7 230.7 %all-reduce.5.cloned.1.call-start = ((), (), s32[]{:S(2)}) async-start(), calls=%async_computation.3 | async-start | bytes 2162688 | tf_op jit(solution)/shard_map/psum | solution.py:18
  203.9 82.7 %all-gather.16.cloned.1.call-start = ((), (), s32[]{:S(2)}) async-start(), calls=%async_computation.5 | async-start | bytes 1824768 | tf_op jit(solution)/shard_map/all_gather | solution.py:84
  204.5 127.3 %all-gather.18.cloned.1.call-start = ((), (), s32[]{:S(2)}) async-start(), calls=%async_computation.6 | async-start | bytes 1824768 | tf_op jit(solution)/shard_map/all_gather | solution.py:85
  205.0 172.0 %all-gather.14.cloned.1.call-start = ((), (), s32[]{:S(2)}) async-start(), calls=%async_computation.4 | async-start | bytes 1824768 | tf_op jit(solution)/shard_map/all_gather | solution.py:83
  205.8 216.6 %all-gather.20.cloned.1.call-start = ((), (), s32[]{:S(2)}) async-start(), calls=%async_computation.7 | async-start | bytes 1824768 | tf_op jit(solution)/shard_map/all_gather | solution.py:86
  206.5 256.0 %all-reduce.7.cloned.1.call-start = ((), (), s32[]{:S(2)}) async-start(), calls=%async_computation.8 | async-start | bytes 2162688 | tf_op jit(solution)/shard_map/psum | solution.py:18
  427.4 83.9 %all-reduce.9.cloned.1.call-start = ((), (), s32[]{:S(2)}) async-start(), calls=%async_computation.9 | async-start | bytes 2162688 | tf_op jit(solution)/shard_map/psum | solution.py:18
  462.6 3.6 copy-start.1
Sparse Core Ops, SparseCore 0:
  9.5 63.7 all-gather.7
  75.5 59.7 all-gather.9
  137.5 59.7 all-gather.11
  204.0 35.3 all-reduce.4
  241.4 45.0 all-gather.15
  288.6 43.0 all-gather.17
  333.9 43.0 all-gather.13
  379.3 43.0 all-gather.19
  427.5 35.0 all-reduce.6
  474.3 37.0 all-reduce.8
where the time goes:
time: 523 us; the launch traced here: 522 us
  waiting for transfers between devices  466 us (89%)
  matrix products  27.7 us (5%)
  other arithmetic  13.6 us (3%)
  between operations  13.6 us (3%)
    psum x3, waiting for transfers between devices, narrow(): lax.psum(partial_value.astype(jnp.bfloat16), 'tp').astype(jnp.float32)  104 us
    all_gather x1, waiting for transfers between devices, local(): lax.all_gather(down_proj, 'fs', axis=0, tiled=True)  62 us
    all_gather x1, waiting for transfers between devices, local(): lax.all_gather(gate_proj, 'fs', axis=0, tiled=True)  61.5 us
    all_gather x1, waiting for transfers between devices, local(): lax.all_gather(up_proj, 'fs', axis=0, tiled=True)  58.7 us
    all_gather x1, waiting for transfers between devices, local(): lax.all_gather(mixer_out, 'fs', axis=0, tiled=True)  45.3 us
    all_gather x1, waiting for transfers between devices, local(): lax.all_gather(inner_gate, 'fs', axis=0, tiled=True)  43.7 us
    all_gather x1, waiting for transfers between devices, local(): lax.all_gather(outer_gate, 'fs', axis=0, tiled=True)  42.9 us
    all_gather x1, waiting for transfers between devices, local(): lax.all_gather(value_proj, 'fs', axis=0, tiled=True)  42.7 us
  transfers between devices with their start and end apart: 10, of which 10 were waited for; matrix products, arithmetic and copies ran while one was open for 3% of the time, Pallas kernels for 0%

commit v1 on v0

--- a/solution.py
+++ b/solution.py
@@ -5,6 +5,11 @@
 
 CONV_K = 3
 EPSILON = 1e-06
+
+
+def _put_stacks_all(state):
+    parts_out = lax.all_gather(state, axis_name="tp")
+    return jnp.sum(parts_out, axis=0)
 
 
 def scaled(values, gain):
@@ -15,7 +20,7 @@
     partial_value = lax.dot_general(
         inner, weight, (((1,), (1,)), ((), ())), preferred_element_type=jnp.float32
     )
-    summed = lax.psum(partial_value.astype(jnp.bfloat16), "tp").astype(jnp.float32)
+    summed = _put_stacks_all(partial_value.astype(jnp.bfloat16)).astype(jnp.float32)
     return (stream.astype(jnp.float32) + factor * scaled(summed, gain)).astype(jnp.bfloat16)
 
 

time: 523 us -> 557 us (1.065)
  local copies, waits for them, and re-layouts: 1.48 us -> 29.2 us
  other arithmetic: 13.6 us -> 40.6 us
  waiting for transfers between devices: 466 us -> 444 us
    psum x3 -> x0, waiting for transfers between devices: 104 us -> none  [narrow(): lax.psum(partial_value.astype(jnp.bfloat16), 'tp').astype(jnp.float32)]
    all_gather x0 -> x3, waiting for transfers between devices: none -> 101 us  [_put_stacks_all(): parts_out = lax.all_gather(state, axis_name='tp')]
    reduce_sum x0 -> x3, other arithmetic: none -> 34.5 us  [_put_stacks_all(): return jnp.sum(parts_out, axis=0)]
    all_gather x0 -> x3, local copies, waits for them, and re-layouts: none -> 26.8 us  [_put_stacks_all(): parts_out = lax.all_gather(state, axis_name='tp')]
    all_gather x1, waiting for transfers between devices: 43.7 us -> 25.4 us  [local(): lax.all_gather(inner_gate, 'fs', axis=0, tiled=True)]
    reduce_sum x6, other arithmetic: 10.1 us -> 3.73 us  [scaled(): jnp.mean(values * values, axis=-1, keepdims=True) + EPSILON]
  transfers between devices with their start and end apart: 10 -> 10, of which waited for: 10 -> 10; matrix products, arithmetic and copies ran while one was open for 3% -> 6% of each run, Pallas kernels for 0% -> 0%
where the time goes in v1:
time: 557 us; the launch traced here: 556 us
  waiting for transfers between devices  444 us (80%)
  other arithmetic  40.6 us (7%)
  local copies, waits for them, and re-layouts  29.2 us (5%)
  matrix products  27.6 us (5%)
  between operations  13.6 us (2%)
    all_gather x3, waiting for transfers between devices, _put_stacks_all(): parts_out = lax.all_gather(state, axis_name='tp')  101 us
    all_gather x1, waiting for transfers between devices, local(): lax.all_gather(down_proj, 'fs', axis=0, tiled=True)  62 us
    all_gather x1, waiting for transfers between devices, local(): lax.all_gather(gate_proj, 'fs', axis=0, tiled=True)  61.5 us
    all_gather x1, waiting for transfers between devices, local(): lax.all_gather(up_proj, 'fs', axis=0, tiled=True)  58.7 us
    all_gather x1, waiting for transfers between devices, local(): lax.all_gather(mixer_out, 'fs', axis=0, tiled=True)  45.3 us
    all_gather x1, waiting for transfers between devices, local(): lax.all_gather(outer_gate, 'fs', axis=0, tiled=True)  42.9 us
    all_gather x1, waiting for transfers between devices, local(): lax.all_gather(value_proj, 'fs', axis=0, tiled=True)  42.7 us
    reduce_sum x3, other arithmetic, _put_stacks_all(): return jnp.sum(parts_out, axis=0)  34.5 us
  transfers between devices with their start and end apart: 10, of which 10 were waited for; matrix products, arithmetic and copies ran while one was open for 6% of the time, Pallas kernels for 0%

profile of v1, /device:TPU:0, one launch (start us, length us, event | category | flops | bytes accessed | tf_op | source)
XLA Modules:
  0.0 555.7 jit_solution(5127036367963951343)
XLA Ops:
  6.5 0.7 all-gather.14.cloned.1.call-update
  7.3 0.7 all-gather.16.cloned.1.call-update
  8.8 1.5 slice_reduce_fusion
  10.2 1.6 fusion.8
  11.8 61.5 %all-gather.14.cloned.1.call-done = bf16[2112,768]{1,0:T(8,128)(2,1)} async-done(((bf16[264,768]{1,0:T(8,128)(2,1)}), bf16[2112,768]{1,0:T(8,128)(2,1)}) %all-gather.14.cloned.1.call-update) | async-done | bytes 3244048 | tf_op jit(solution)/shard_map/all_gather | solution.py:81
  73.3 3.2 fusion.36
  76.5 58.7 %all-gather.16.cloned.1.call-done = bf16[2112,768]{1,0:T(8,128)(2,1)} async-done(((bf16[264,768]{1,0:T(8,128)(2,1)}), bf16[2112,768]{1,0:T(8,128)(2,1)}) %all-gather.16.cloned.1.call-update) | async-done | bytes 3244048 | tf_op jit(solution)/shard_map/all_gather | solution.py:82
  135.3 62.0 %all-gather.18.cloned.1.call-done = bf16[2112,768]{1,0:T(8,128)(2,1)} async-done(((bf16[264,768]{1,0:T(8,128)(2,1)}), bf16[2112,768]{1,0:T(8,128)(2,1)}) %all-gather.18.cloned.1.call-update) | async-done | bytes 3244048 | tf_op jit(solution)/shard_map/all_gather | solution.py:83
  197.2 6.6 %convolution_convert_fusion.2 = bf16[256,2112]{0,1:T(8,128)(2,1)} fusion(bf16[2112,768]{1,0:T(8,128)(2,1)} %all-gather.18.cloned.1.call-done, bf16[2112,768]{1,0:T(8,128)(2,1)} %all-gather.16.cloned.1.call-done, f32[256,768]{1,0:T(8,128)S(1)} %fusion.36, bf16[256,2112]{0,1:T(8,128)(2,1)S(1)} %copy-done, f32[2112]{0:T(1024)S(1)} %get-tuple-element.9, ...), kind=kOutput, calls=%fused_computation.2 | convolution fusion | flops 1664827392 | bytes 9446656 | tf_op jit(solution)/shard_map/dot_general | solution.py:20
  205.1 0.7 all-gather.20.cloned.1.call-update
  205.8 0.7 all-gather.26.cloned.1.call-update
  206.8 0.8 dynamic-slice_convert_fusion
  207.6 30.9 %all-gather.28.cloned.1.call-done = bf16[1024,2112]{0,1:T(8,128)(2,1)} async-done(((bf16[256,2112]{0,1:T(8,128)(2,1)}), bf16[1024,2112]{0,1:T(8,128)(2,1)}) %all-gather.28.cloned.1.call-update) | async-done | bytes 4325392 | tf_op jit(solution)/shard_map/all_gather | solution.py:11
  238.5 8.9 %reshape.48 = bf16[4,256,2112]{1,0,2:T(4,128)(2,1)} reshape(bf16[1024,2112]{0,1:T(8,128)(2,1)} %all-gather.28.cloned.1.call-done) | data formatting | bytes 8650752 | tf_op jit(solution)/shard_map/all_gather | solution.py:11
  247.4 11.5 %reduce_sum.91 = bf16[256,2112]{0,1:T(8,128)(2,1)S(1)} reduce(bf16[4,256,2112]{1,0,2:T(4,128)(2,1)} %reshape.48, bf16[]{:T(256)} %constant.27.clone.1), dimensions={0}, to_apply=%region_1.2 | reduce | flops 1622016 | bytes 5406722 | tf_op jit(solution)/shard_map/reduce_sum | solution.py:12
  259.9 25.4 %all-gather.22.cloned.1.call-done = bf16[2112,264]{1,0:T(8,128)(2,1)} async-done(((bf16[264,264]{1,0:T(8,128)(2,1)}), bf16[2112,264]{1,0:T(8,128)(2,1)}) %all-gather.22.cloned.1.call-update) | async-done | bytes 1115152 | tf_op jit(solution)/shard_map/all_gather | solution.py:89
  285.3 2.4 fusion.24
  287.7 42.7 %all-gather.24.cloned.1.call-done = bf16[2112,264]{1,0:T(8,128)(2,1)} async-done(((bf16[264,264]{1,0:T(8,128)(2,1)}), bf16[2112,264]{1,0:T(8,128)(2,1)}) %all-gather.24.cloned.1.call-update) | async-done | bytes 1115152 | tf_op jit(solution)/shard_map/all_gather | solution.py:90
  330.5 2.4 fusion.23
  332.9 42.9 %all-gather.20.cloned.1.call-done = bf16[2112,264]{1,0:T(8,128)(2,1)} async-done(((bf16[264,264]{1,0:T(8,128)(2,1)}), bf16[2112,264]{1,0:T(8,128)(2,1)}) %all-gather.20.cloned.1.call-update) | async-done | bytes 1115152 | tf_op jit(solution)/shard_map/all_gather | solution.py:88
  375.8 45.3 %all-gather.26.cloned.1.call-done = bf16[2112,264]{1,0:T(8,128)(2,1)} async-done(((bf16[264,264]{1,0:T(8,128)(2,1)}), bf16[2112,264]{1,0:T(8,128)(2,1)}) %all-gather.26.cloned.1.call-update) | async-done | bytes 1115152 | tf_op jit(solution)/shard_map/all_gather | solution.py:91
  421.1 4.9 convolution_convert_fusion.1
  426.1 34.2 %all-gather.30.cloned.1.call-done = bf16[1024,2112]{0,1:T(8,128)(2,1)} async-done(((bf16[256,2112]{0,1:T(8,128)(2,1)}), bf16[1024,2112]{0,1:T(8,128)(2,1)}) %all-gather.30.cloned.1.call-update) | async-done | bytes 4325392 | tf_op jit(solution)/shard_map/all_gather | solution.py:11
  460.3 8.9 %reshape.49 = bf16[4,256,2112]{1,0,2:T(4,128)(2,1)} reshape(bf16[1024,2112]{0,1:T(8,128)(2,1)} %all-gather.30.cloned.1.call-done) | data formatting | bytes 8650752 | tf_op jit(solution)/shard_map/all_gather | solution.py:11
  469.3 11.5 %reduce_sum.94 = bf16[256,2112]{0,1:T(8,128)(2,1)S(1)} reduce(bf16[4,256,2112]{1,0,2:T(4,128)(2,1)} %reshape.49, bf16[]{:T(256)} %constant.27.clone.1), dimensions={0}, to_apply=%region_4.5 | reduce | flops 1622016 | bytes 5406722 | tf_op jit(solution)/shard_map/reduce_sum | solution.py:12
  481.7 1.0 copy-done.1
  482.7 1.4 fusion.32
  484.0 6.6 %convolution_convert_fusion = bf16[256,2112]{0,1:T(8,128)(2,1)} fusion(bf16[2112,768]{1,0:T(8,128)(2,1)} %all-gather.18.cloned.1.call-done, bf16[2112,768]{1,0:T(8,128)(2,1)} %all-gather.16.cloned.1.call-done, f32[256,768]{1,0:T(8,128)S(1)} %fusion.32, bf16[256,2112]{0,1:T(8,128)(2,1)S(1)} %get-tuple-element.15, f32[2112]{0:T(1024)S(1)} %get-tuple-element.10, ...), kind=kOutput, calls=%fused_computation | convolution fusion | flops 1664827392 | bytes 9446656 | tf_op jit(solution)/shard_map/dot_general | solution.py:20
  490.7 35.9 %all-gather.32.cloned.1.call-done = bf16[1024,2112]{0,1:T(8,128)(2,1)} async-done(((bf16[256,2112]{0,1:T(8,128)(2,1)}), bf16[1024,2112]{0,1:T(8,128)(2,1)}) %all-gather.32.cloned.1.call-update) | async-done | bytes 4325392 | tf_op jit(solution)/shard_map/all_gather | solution.py:11
  526.6 8.9 %reshape.50 = bf16[4,256,2112]{1,0,2:T(4,128)(2,1)} reshape(bf16[1024,2112]{0,1:T(8,128)(2,1)} %all-gather.32.cloned.1.call-done) | data formatting | bytes 8650752 | tf_op jit(solution)/shard_map/all_gather | solution.py:11
  535.5 11.5 %reduce_sum.97 = bf16[256,2112]{0,1:T(8,128)(2,1)S(1)} reduce(bf16[4,256,2112]{1,0,2:T(4,128)(2,1)} %reshape.50, bf16[]{:T(256)} %constant.27.clone.1), dimensions={0}, to_apply=%region_7.8 | reduce | flops 1622016 | bytes 5406722 | tf_op jit(solution)/shard_map/reduce_sum | solution.py:12
  547.4 1.5 fusion.19
  (31 shorter events, 4.6 us)
Async XLA Ops:
  6.5 66.8 %copy-start = (bf16[256,2112]{0,1:T(8,128)(2,1)S(1)}, bf16[256,2112]{0,1:T(8,128)(2,1)}, u32[]{:S(2)}) copy-start(bf16[256,2112]{0,1:T(8,128)(2,1)} %param.10) | copy-start | bytes 3244036
  6.5 66.8 %all-gather.14.cloned.1.call-start = ((), (), s32[]{:S(2)}) async-start(), calls=%async_computation | async-start | bytes 3649536 | tf_op jit(solution)/shard_map/all_gather | solution.py:81
  7.3 128.0 %all-gather.16.cloned.1.call-start = ((), (), s32[]{:S(2)}) async-start(), calls=%async_computation.1 | async-start | bytes 3649536 | tf_op jit(solution)/shard_map/all_gather | solution.py:82
  8.0 189.2 %all-gather.18.cloned.1.call-start = ((), (), s32[]{:S(2)}) async-start(), calls=%async_computation.2 | async-start | bytes 3649536 | tf_op jit(solution)/shard_map/all_gather | solution.py:83
  8.7 229.7 %all-gather.28.cloned.1.call-start = ((), (), s32[]{:S(2)}) async-start(), calls=%async_computation.7 | async-start | bytes 5406720 | tf_op jit(solution)/shard_map/all_gather | solution.py:11
  203.9 81.4 %all-gather.22.cloned.1.call-start = ((), (), s32[]{:S(2)}) async-start(), calls=%async_computation.4 | async-start | bytes 1824768 | tf_op jit(solution)/shard_map/all_gather | solution.py:89
  204.5 126.0 %all-gather.24.cloned.1.call-start = ((), (), s32[]{:S(2)}) async-start(), calls=%async_computation.5 | async-start | bytes 1824768 | tf_op jit(solution)/shard_map/all_gather | solution.py:90
  205.0 170.8 %all-gather.20.cloned.1.call-start = ((), (), s32[]{:S(2)}) async-start(), calls=%async_computation.3 | async-start | bytes 1824768 | tf_op jit(solution)/shard_map/all_gather | solution.py:88
  205.8 215.3 %all-gather.26.cloned.1.call-start = ((), (), s32[]{:S(2)}) async-start(), calls=%async_computation.6 | async-start | bytes 1824768 | tf_op jit(solution)/shard_map/all_gather | solution.py:91
  206.5 253.8 %all-gather.30.cloned.1.call-start = ((), (), s32[]{:S(2)}) async-start(), calls=%async_computation.8 | async-start | bytes 5406720 | tf_op jit(solution)/shard_map/all_gather | solution.py:11
  426.1 100.5 %all-gather.32.cloned.1.call-start = ((), (), s32[]{:S(2)}) async-start(), calls=%async_computation.9 | async-start | bytes 5406720 | tf_op jit(solution)/shard_map/all_gather | solution.py:11
  480.8 1.9 copy-start.1
Sparse Core Ops, SparseCore 0:
  9.5 63.7 all-gather.13
  75.5 59.7 all-gather.15
  137.4 59.7 all-gather.17
  204.0 34.4 all-gather.27
  240.5 44.7 all-gather.21
  287.3 43.0 all-gather.23
  332.7 43.0 all-gather.19
  378.0 43.0 all-gather.25
  426.2 34.0 all-gather.29
  490.8 35.7 all-gather.31
